TPU v7x, 256 devices: a whole 4x4x8 slice. The times are simulated.
256 devices in a mesh: kv: 32 (over z, y), tp: 8 (over x, core).
Axes of the slice: x: 4, y: 4, z: 8, core: 2. Of those that a mesh axis runs over, the one named last changes fastest.
Arguments:
- residual_in: bfloat16 [256, 2048], P(None, ('kv', 'tp')), may hold values from -14 to 14
- delta_state: float32 [256, 32, 128, 128], P('kv', 'tp'), may hold values from -1 to 1
- norm_gain_first: float32 [2048], P('kv'), may hold values from 0.1 to 1.9
- gate_first: bfloat16 [2048, 5632], P('kv', 'tp'), may hold values from -0.125 to 0.125
- up_first: bfloat16 [2048, 5632], P('kv', 'tp'), may hold values from -0.125 to 0.125
- down_first: bfloat16 [5632, 2048], P('tp', 'kv'), may hold values from -0.15625 to 0.15625
- norm_gain_mixer: float32 [2048], P('kv'), may hold values from 0.1 to 1.9
- query_weight: bfloat16 [2048, 2048], P('kv', 'tp'), may hold values from -0.125 to 0.125
- key_weight: bfloat16 [2048, 2048], P('kv', 'tp'), may hold values from -0.125 to 0.125
- value_weight: bfloat16 [2048, 4096], P('kv', 'tp'), may hold values from -0.125 to 0.125
- output_gate_weight: bfloat16 [2048, 4096], P('kv', 'tp'), may hold values from -0.125 to 0.125
- beta_weight: bfloat16 [2048, 32], P('kv'), may hold values from -0.125 to 0.125
- decay_weight: bfloat16 [2048, 32], P('kv'), may hold values from -0.125 to 0.125
- decay_rate: float32 [32], P('tp'), may hold values from -2.3 to 1.1
- decay_bias: float32 [32], P('tp'), may hold values from -1 to 1
- head_gain: float32 [128], replicated, may hold values from 0.1 to 1.9
- out_weight: bfloat16 [4096, 2048], P('tp', 'kv'), may hold values from -0.125 to 0.125
- norm_gain_second: float32 [2048], P('kv'), may hold values from 0.1 to 1.9
- gate_second: bfloat16 [2048, 5632], P('kv', 'tp'), may hold values from -0.125 to 0.125
- up_second: bfloat16 [2048, 5632], P('kv', 'tp'), may hold values from -0.125 to 0.125
- down_second: bfloat16 [5632, 2048], P('tp', 'kv'), may hold values from -0.15625 to 0.15625
Outputs:
- residual_out: bfloat16 [256, 2048], P(None, ('kv', 'tp'))
- delta_state_out: float32 [256, 32, 128, 128], P('kv', 'tp')
All inputs are finite; a program needn't handle non-finite values.
Results may differ from a plain program's by a relative error of at most 0.03.
Values may be sent and summed in bfloat16 or wider, within the bound.
A program may use at most 64 MiB of HBM per device.

v0:
```python
import jax
import jax.numpy as jnp
from jax import lax
from jax.sharding import PartitionSpec as P

D = 2048
epsilon = 1e-06


def in_blocks(value, dim, size):
    before, after = (value.shape[:dim], value.shape[dim + 1 :])
    return jnp.moveaxis(value.reshape(*before, size, -1, *after), dim, 0)


def summed_on_arrival(value, axis, dim):
    blocks = in_blocks(value, dim, lax.axis_size(axis))
    arrived = lax.all_to_all(blocks, axis, split_axis=0, concat_axis=0, tiled=True)
    return arrived.astype(jnp.float32).sum(axis=0)


def side_by_side(arrays, axis, dim, along):
    columns = [a.reshape(*a.shape[:along], -1) for a in arrays]
    both = jnp.concatenate(columns, axis=along)
    result, at, outs = (summed_on_arrival(both, axis, dim), 0, [])
    for a, column in zip(arrays, columns):
        piece = result[..., at : at + column.shape[along]]
        outs.append(piece.reshape(*piece.shape[:along], *a.shape[along:]))
        at += column.shape[along]
    return tuple(outs)


def joined_along(blocks, dim):
    dims = list(blocks.shape[1:])
    dims[dim] *= blocks.shape[0]
    return jnp.moveaxis(blocks, 0, dim).reshape(dims)


def from_everyone(value, axis):
    copies = jnp.broadcast_to(value, (lax.axis_size(axis), *value.shape))
    return lax.all_to_all(copies, axis, split_axis=0, concat_axis=0, tiled=True)


def collect(value, axis, dim):
    return joined_along(from_everyone(value, axis), dim)


def activate(summed, square_sums, hidden_cols):
    rowscale = lax.rsqrt(square_sums / D + epsilon)[:, None]
    gate_act = summed[:, :hidden_cols] * rowscale
    up_act = summed[:, hidden_cols:] * rowscale
    return (jax.nn.silu(gate_act) * up_act).astype(jnp.bfloat16)


def feed_forward(residual, norm_gain, gate_weight, up_weight, down_weight, finish):
    as_float = residual.astype(jnp.float32)
    squares = jnp.sum(as_float * as_float, axis=1)
    scaled = (as_float * norm_gain).astype(jnp.bfloat16)
    joined = jnp.concatenate([gate_weight, up_weight], axis=1)
    partial_value = jnp.dot(scaled, joined, preferred_element_type=jnp.float32)
    hidden_cols = gate_weight.shape[1]
    summed, square_sums = side_by_side(
        (partial_value.astype(jnp.bfloat16), squares.astype(jnp.bfloat16)), "kv", 0, 1
    )
    hidden = activate(summed, square_sums, hidden_cols)
    projected = jnp.dot(
        collect(hidden, "kv", 0), down_weight, preferred_element_type=jnp.float32
    ).astype(jnp.bfloat16)
    if finish:
        col_count = residual.shape[1] // lax.axis_size("tp")
        own_cols = lax.dynamic_slice_in_dim(
            as_float, lax.axis_index("tp") * col_count, col_count, 1
        )
        branch = summed_on_arrival(projected, "tp", 1)
        return (own_cols + 0.5 * branch).astype(jnp.bfloat16)
    branch = lax.psum(projected, "tp").astype(jnp.float32)
    return (as_float + 0.5 * branch).astype(jnp.bfloat16)


def unit_heads(projected, head_size):
    activated = jax.nn.silu(projected).reshape(projected.shape[0], -1, head_size)
    return activated * lax.rsqrt(jnp.sum(activated * activated, axis=-1, keepdims=True) + epsilon)


def delta_step(old_state, key_rows, queries, values, beta_gate, decay_gate):
    faded_state = old_state * decay_gate[:, :, None, None]
    predicted = jnp.einsum("rhab,rha->rhb", faded_state, key_rows, precision=lax.Precision.HIGHEST)
    correction = beta_gate[:, :, None] * (values - predicted)
    updated = faded_state + key_rows[:, :, :, None] * correction[:, :, None, :]
    reading = jnp.einsum("rhab,rha->rhb", updated, queries, precision=lax.Precision.HIGHEST)
    return (updated, reading)


def token_mixer(
    residual,
    norm_gain,
    query_weight,
    key_weight,
    value_weight,
    output_gate_weight,
    beta_weight,
    decay_weight,
    decay_rate,
    decay_bias,
    head_gain,
    out_weight,
    old_state,
):
    as_float = residual.astype(jnp.float32)
    squares = jnp.sum(as_float * as_float, axis=1)
    scaled = (as_float * norm_gain).astype(jnp.bfloat16)
    joined = jnp.concatenate([query_weight, key_weight, value_weight, output_gate_weight], axis=1)
    partial_value = jnp.dot(scaled, joined, preferred_element_type=jnp.float32)
    heads_dev = decay_rate.shape[0]
    head_start = lax.axis_index("tp") * heads_dev
    gate_cols = jnp.concatenate(
        [
            lax.dynamic_slice_in_dim(beta_weight, head_start, heads_dev, 1),
            lax.dynamic_slice_in_dim(decay_weight, head_start, heads_dev, 1),
        ],
        axis=1,
    )
    gate_part = jnp.dot(scaled, gate_cols, preferred_element_type=jnp.float32)
    row_count = old_state.shape[0]
    summed, gate_summed, square_sums = side_by_side(
        (
            partial_value.astype(jnp.bfloat16),
            gate_part.astype(jnp.bfloat16),
            squares.astype(jnp.bfloat16),
        ),
        "kv",
        0,
        1,
    )
    rowscale = lax.rsqrt(square_sums / D + epsilon)[:, None]
    summed = summed * rowscale
    gate_summed = gate_summed * rowscale
    head_size = old_state.shape[2]
    key_cols = query_weight.shape[1]
    value_cols = value_weight.shape[1]
    repeat_count = heads_dev // (key_cols // head_size)
    queries = jnp.repeat(
        unit_heads(summed[:, :key_cols], head_size) * head_size ** (-0.5), repeat_count, axis=1
    )
    key_rows = jnp.repeat(
        unit_heads(summed[:, key_cols : 2 * key_cols], head_size), repeat_count, axis=1
    )
    values = jax.nn.silu(summed[:, 2 * key_cols : 2 * key_cols + value_cols]).reshape(
        row_count, heads_dev, head_size
    )
    out_gate = jax.nn.silu(summed[:, 2 * key_cols + value_cols :]).reshape(
        row_count, heads_dev, head_size
    )
    beta_gate = jax.nn.sigmoid(gate_summed[:, :heads_dev])
    decay_gate = jnp.exp(
        -jnp.exp(decay_rate)[None, :]
        * jax.nn.softplus(gate_summed[:, heads_dev:] + decay_bias[None, :])
    )
    new_state, reading = delta_step(old_state, key_rows, queries, values, beta_gate, decay_gate)
    normed = reading * lax.rsqrt(jnp.mean(reading * reading, axis=-1, keepdims=True) + epsilon)
    normed = (
        (normed * head_gain * out_gate)
        .reshape(row_count, heads_dev * head_size)
        .astype(jnp.bfloat16)
    )
    projected = jnp.dot(
        collect(normed, "kv", 0), out_weight, preferred_element_type=jnp.float32
    ).astype(jnp.bfloat16)
    branch = lax.psum(projected, "tp").astype(jnp.float32)
    return ((as_float + branch).astype(jnp.bfloat16), new_state)


def body(
    residual_in,
    delta_state,
    norm_gain_first,
    gate_first,
    up_first,
    down_first,
    norm_gain_mixer,
    query_weight,
    key_weight,
    value_weight,
    output_gate_weight,
    beta_weight,
    decay_weight,
    decay_rate,
    decay_bias,
    head_gain,
    out_weight,
    norm_gain_second,
    gate_second,
    up_second,
    down_second,
):
    columns = lax.all_gather(residual_in, "tp", axis=1, tiled=True)
    after_first = feed_forward(columns, norm_gain_first, gate_first, up_first, down_first, False)
    after_mixer, new_state = token_mixer(
        after_first,
        norm_gain_mixer,
        query_weight,
        key_weight,
        value_weight,
        output_gate_weight,
        beta_weight,
        decay_weight,
        decay_rate,
        decay_bias,
        head_gain,
        out_weight,
        delta_state,
    )
    residual_out = feed_forward(
        after_mixer, norm_gain_second, gate_second, up_second, down_second, True
    )
    return (residual_out, new_state)


def solution(mesh):
    placed = (
        P(None, ("kv", "tp")),
        P("kv", "tp", None, None),
        P("kv"),
        P("kv", "tp"),
        P("kv", "tp"),
        P("tp", "kv"),
        P("kv"),
        P("kv", "tp"),
        P("kv", "tp"),
        P("kv", "tp"),
        P("kv", "tp"),
        P("kv", None),
        P("kv", None),
        P("tp"),
        P("tp"),
        P(),
        P("tp", "kv"),
        P("kv"),
        P("kv", "tp"),
        P("kv", "tp"),
        P("tp", "kv"),
    )
    return jax.shard_map(
        body,
        mesh=mesh,
        in_specs=placed,
        out_specs=(P(None, ("kv", "tp")), P("kv", "tp", None, None)),
        check_vma=False,
    )
```

profile of v0, /device:TPU:1, one launch (start us, length us, event | category | flops | bytes accessed | tf_op | source)
XLA Modules:
  0.0 230.6 jit_solution(4892839816095156955)
XLA Ops:
  0.6 16.2 %all_gather.3 = bf16[256,64]{0,1:T(8,128)(2,1)S(1)} all-gather(bf16[256,8]{0,1:T(8,128)(2,1)} %param.21), channel_id=1, replica_groups=mesh['kv'=32,'tp'=8] {'tp'}, dimensions={1}, use_global_device_ids=true | all-gather | bytes 36864 | tf_op jit(solution)/shard_map/all_gather | solution.py:195
  17.1 1.4 fusion
  18.7 31.4 %all_to_all.35 = bf16[32,8,1409]{2,1,0:T(8,128)(2,1)S(1)} all-to-all(bf16[32,8,1409]{2,1,0:T(8,128)(2,1)S(1)} %pad_maximum_fusion), channel_id=1, replica_groups=mesh['kv'=32,'tp'=8] {'kv'}, dimensions={0} | all-to-all | bytes 1442816 | tf_op jit(solution)/shard_map/all_to_all | solution.py:17
  50.4 0.8 broadcast_in_dim.10
  51.2 5.6 %all-to-all-start.1 = ((bf16[32,8,704]{2,1,0:T(8,128)(2,1)}), bf16[32,8,704]{2,1,0:T(8,128)(2,1)S(1)}, u32[]{:S(2)}, u32[]{:S(2)}) async-start(bf16[32,8,704]{2,1,0:T(8,128)(2,1)} %broadcast_in_dim.10), calls=%async_computation.1 | async-start | bytes 786432 | tf_op jit(solution)/shard_map/all_to_all | solution.py:40
  56.8 0.7 constant_dynamic-slice_fusion
  57.5 12.1 %all-to-all-done.1 = bf16[32,8,704]{2,1,0:T(8,128)(2,1)S(1)} async-done(((bf16[32,8,704]{2,1,0:T(8,128)(2,1)}), bf16[32,8,704]{2,1,0:T(8,128)(2,1)S(1)}, u32[]{:S(2)}, u32[]{:S(2)}) %all-to-all-start.1) | async-done | bytes 360480 | tf_op jit(solution)/shard_map/all_to_all | solution.py:40
  69.8 23.5 %psum.14 = bf16[256,64]{0,1:T(8,128)(2,1)S(1)} all-reduce(bf16[256,64]{0,1:T(8,128)(2,1)S(1)} %convolution_convert_fusion.5), channel_id=1, replica_groups=mesh['kv'=32,'tp'=8] {'tp'}, use_global_device_ids=true, to_apply=%region_2.3 | all-reduce | flops 16384 | bytes 65536 | tf_op jit(solution)/shard_map/psum | solution.py:75
  94.0 0.5 fusion.1
  94.5 1.1 concatenate.39
  95.6 4.6 %all-to-all-start.2 = ((bf16[32,8,1545]{2,1,0:T(8,128)(2,1)}), bf16[32,8,1545]{2,1,0:T(8,128)(2,1)S(1)}, u32[]{:S(2)}, u32[]{:S(2)}) async-start(bf16[32,8,1545]{2,1,0:T(8,128)(2,1)} %concatenate.39), calls=%async_computation.2 | async-start | bytes 1703936 | tf_op jit(solution)/shard_map/all_to_all | solution.py:17
  100.3 19.5 %all-to-all-done.2 = bf16[32,8,1545]{2,1,0:T(8,128)(2,1)S(1)} async-done(((bf16[32,8,1545]{2,1,0:T(8,128)(2,1)}), bf16[32,8,1545]{2,1,0:T(8,128)(2,1)S(1)}, u32[]{:S(2)}, u32[]{:S(2)}) %all-to-all-start.2) | async-done | bytes 791072 | tf_op jit(solution)/shard_map/all_to_all | solution.py:17
  120.6 2.0 fusion.3
  122.7 0.7 multiply_add_fusion
  123.6 1.2 copy-done.2
  124.8 1.9 fusion.67
  126.9 17.3 %all_to_all.36 = bf16[32,8,512]{2,1,0:T(8,128)(2,1)S(1)} all-to-all(bf16[32,8,512]{2,1,0:T(8,128)(2,1)S(1)} %broadcast_in_dim.13), channel_id=1, replica_groups=mesh['kv'=32,'tp'=8] {'kv'}, dimensions={0} | all-to-all | bytes 524288 | tf_op jit(solution)/shard_map/all_to_all | solution.py:40
  144.4 26.0 %psum.15 = bf16[256,64]{0,1:T(8,128)(2,1)S(1)} all-reduce(bf16[256,64]{0,1:T(8,128)(2,1)S(1)} %convolution_convert_fusion.3), channel_id=1, replica_groups=mesh['kv'=32,'tp'=8] {'tp'}, use_global_device_ids=true, to_apply=%region_8.9 | all-reduce | flops 16384 | bytes 65536 | tf_op jit(solution)/shard_map/psum | solution.py:168
  171.2 22.8 %all_to_all.37 = bf16[32,8,1409]{2,1,0:T(8,128)(2,1)S(1)} all-to-all(bf16[32,8,1409]{2,1,0:T(8,128)(2,1)S(1)} %pad_maximum_fusion.1), channel_id=1, replica_groups=mesh['kv'=32,'tp'=8] {'kv'}, dimensions={0} | all-to-all | bytes 1442816 | tf_op jit(solution)/shard_map/all_to_all | solution.py:17
  194.4 18.7 %all_to_all.38 = bf16[32,8,704]{2,1,0:T(8,128)(2,1)S(1)} all-to-all(bf16[32,8,704]{2,1,0:T(8,128)(2,1)S(1)} %broadcast_in_dim.14), channel_id=1, replica_groups=mesh['kv'=32,'tp'=8] {'kv'}, dimensions={0} | all-to-all | bytes 720896 | tf_op jit(solution)/shard_map/all_to_all | solution.py:40
  213.1 0.9 fusion.5
  214.0 11.3 %all-to-all-start.6 = ((bf16[8,256,8]{1,2,0:T(8,128)(2,1)}), bf16[8,256,8]{1,2,0:T(8,128)(2,1)S(1)}, u32[]{:S(2)}, u32[]{:S(2)}) async-start(bf16[8,256,8]{1,2,0:T(8,128)(2,1)} %fusion.5), calls=%async_computation.6 | async-start | bytes 65536 | tf_op jit(solution)/shard_map/all_to_all | solution.py:17
  225.2 4.7 %all-to-all-done.6 = bf16[8,256,8]{1,2,0:T(8,128)(2,1)S(1)} async-done(((bf16[8,256,8]{1,2,0:T(8,128)(2,1)}), bf16[8,256,8]{1,2,0:T(8,128)(2,1)S(1)}, u32[]{:S(2)}, u32[]{:S(2)}) %all-to-all-start.6) | async-done | bytes 32800 | tf_op jit(solution)/shard_map/all_to_all | solution.py:17
  230.0 0.6 add_convert_fusion
  (73 shorter events, 4.1 us)
Async XLA Ops:
  0.6 68.9 %copy-start = (bf16[704,64]{0,1:T(8,128)(2,1)S(1)}, bf16[704,64]{0,1:T(8,128)(2,1)}, u32[]{:S(2)}) copy-start(bf16[704,64]{0,1:T(8,128)(2,1)} %param.26) | copy-start | bytes 270340
  18.6 74.8 %copy-start.11 = (f32[64]{0:T(128)S(1)}, f32[64]{0:T(128)}, u32[]{:S(2)}) copy-start(f32[64]{0:T(128)} %param.27) | copy-start | bytes 772
  18.6 75.4 %copy-start.6 = (bf16[64,512]{1,0:T(8,128)(2,1)S(1)}, bf16[64,512]{1,0:T(8,128)(2,1)}, u32[]{:S(2)}) copy-start(bf16[64,512]{1,0:T(8,128)(2,1)} %param.31) | copy-start | bytes 196612
  18.6 75.4 %copy-start.7 = (bf16[64,512]{1,0:T(8,128)(2,1)S(1)}, bf16[64,512]{1,0:T(8,128)(2,1)}, u32[]{:S(2)}) copy-start(bf16[64,512]{1,0:T(8,128)(2,1)} %param.30) | copy-start | bytes 196612
  18.6 75.4 %copy-start.9 = (bf16[64,256]{1,0:T(8,128)(2,1)S(1)}, bf16[64,256]{1,0:T(8,128)(2,1)}, u32[]{:S(2)}) copy-start(bf16[64,256]{1,0:T(8,128)(2,1)} %param.29) | copy-start | bytes 98308
  18.7 75.4 %copy-start.10 = (bf16[64,256]{1,0:T(8,128)(2,1)S(1)}, bf16[64,256]{1,0:T(8,128)(2,1)}, u32[]{:S(2)}) copy-start(bf16[64,256]{1,0:T(8,128)(2,1)} %param.28) | copy-start | bytes 98308
  51.2 18.4 %all-to-all-start.1 = ((bf16[32,8,704]{2,1,0:T(8,128)(2,1)}), bf16[32,8,704]{2,1,0:T(8,128)(2,1)S(1)}, u32[]{:S(2)}, u32[]{:S(2)}) async-start(bf16[32,8,704]{2,1,0:T(8,128)(2,1)} %broadcast_in_dim.10), calls=%async_computation.1 | async-start | bytes 786432 | tf_op jit(solution)/shard_map/all_to_all | solution.py:40
  94.0 6.2 %copy-start.15 = (f32[4]{0:T(128)S(1)}, f32[4]{0:T(128)}, u32[]{:S(2)}) copy-start(f32[4]{0:T(128)} %param.34) | copy-start | bytes 52
  94.5 25.8 %copy-start.14 = (f32[4]{0:T(128)S(1)}, f32[4]{0:T(128)}, u32[]{:S(2)}) copy-start(f32[4]{0:T(128)} %param.35) | copy-start | bytes 52
  94.5 26.1 %copy-start.1 = (f32[8,4,128,128]{3,2,1,0:T(8,128)S(1)}, f32[8,4,128,128]{3,2,1,0:T(8,128)}, u32[]{:S(2)}) copy-start(f32[8,4,128,128]{3,2,1,0:T(8,128)} %param.22) | copy-start | bytes 6291460
  95.6 24.1 %all-to-all-start.2 = ((bf16[32,8,1545]{2,1,0:T(8,128)(2,1)}), bf16[32,8,1545]{2,1,0:T(8,128)(2,1)S(1)}, u32[]{:S(2)}, u32[]{:S(2)}) async-start(bf16[32,8,1545]{2,1,0:T(8,128)(2,1)} %concatenate.39), calls=%async_computation.2 | async-start | bytes 1703936 | tf_op jit(solution)/shard_map/all_to_all | solution.py:17
  123.5 1.3 copy-start.2
  123.5 3.3 %copy-start.13 = (f32[128]{0:T(128)S(1)}, f32[128]{0:T(128)}, u32[]{:S(2)}) copy-start(f32[128]{0:T(128)} %param.36) | copy-start | bytes 1540
  123.5 20.7 %copy-start.8 = (bf16[512,64]{0,1:T(8,128)(2,1)S(1)}, bf16[512,64]{0,1:T(8,128)(2,1)}, u32[]{:S(2)}) copy-start(bf16[512,64]{0,1:T(8,128)(2,1)} %param.37) | copy-start | bytes 196612
  123.5 47.1 %copy-start.3 = (bf16[64,704]{1,0:T(8,128)(2,1)S(1)}, bf16[64,704]{1,0:T(8,128)(2,1)}, u32[]{:S(2)}) copy-start(bf16[64,704]{1,0:T(8,128)(2,1)} %param.40) | copy-start | bytes 270340
  123.5 47.1 %copy-start.4 = (bf16[64,704]{1,0:T(8,128)(2,1)S(1)}, bf16[64,704]{1,0:T(8,128)(2,1)}, u32[]{:S(2)}) copy-start(bf16[64,704]{1,0:T(8,128)(2,1)} %param.39) | copy-start | bytes 270340
  123.5 47.1 %copy-start.12 = (f32[64]{0:T(128)S(1)}, f32[64]{0:T(128)}, u32[]{:S(2)}) copy-start(f32[64]{0:T(128)} %param.38) | copy-start | bytes 772
  171.2 41.9 %copy-start.5 = (bf16[704,64]{0,1:T(8,128)(2,1)S(1)}, bf16[704,64]{0,1:T(8,128)(2,1)}, u32[]{:S(2)}) copy-start(bf16[704,64]{0,1:T(8,128)(2,1)} %param.41) | copy-start | bytes 270340
  214.0 16.0 %all-to-all-start.6 = ((bf16[8,256,8]{1,2,0:T(8,128)(2,1)}), bf16[8,256,8]{1,2,0:T(8,128)(2,1)S(1)}, u32[]{:S(2)}, u32[]{:S(2)}) async-start(bf16[8,256,8]{1,2,0:T(8,128)(2,1)} %fusion.5), calls=%async_computation.6 | async-start | bytes 65536 | tf_op jit(solution)/shard_map/all_to_all | solution.py:17
where the time goes:
time: 231 us
  blocking collectives  156 us (68%)
  waiting for transfers between devices  36.3 us (16%)
  starting transfers between devices  21.5 us (9%)
  matrix products  7.71 us (3%)
  local copies, waits for them, and re-layouts  4.91 us (2%)
  other arithmetic  3.23 us (1%)
    all_to_all x2, blocking collectives, summed_on_arrival(): lax.all_to_all(blocks, axis, split_axis=0, concat_axis=0, tiled=True)  54.2 us
    all_to_all x2, blocking collectives, from_everyone(): return lax.all_to_all(copies, axis, split_axis=0, concat_axis=0, tiled=True)  36 us
    psum x1, blocking collectives, token_mixer(): branch = lax.psum(projected, 'tp').astype(jnp.float32)  26 us
    all_to_all x2, waiting for transfers between devices, summed_on_arrival(): lax.all_to_all(blocks, axis, split_axis=0, concat_axis=0, tiled=True)  24.2 us
    psum x1, blocking collectives, feed_forward(): branch = lax.psum(projected, 'tp').astype(jnp.float32)  23.5 us
    all_gather x1, blocking collectives, body(): columns = lax.all_gather(residual_in, 'tp', axis=1, tiled=True)  16.2 us
    all_to_all x2, starting transfers between devices, summed_on_arrival(): lax.all_to_all(blocks, axis, split_axis=0, concat_axis=0, tiled=True)  15.9 us
    all_to_all x1, waiting for transfers between devices, from_everyone(): return lax.all_to_all(copies, axis, split_axis=0, concat_axis=0, tiled=True)  12.1 us
  transfers between devices with their start and end apart: 3, of which 3 were waited for; matrix products, arithmetic and copies ran while one was open for 0% of the time, Pallas kernels for 0%

commit v1 on v0

--- a/solution.py
+++ b/solution.py
@@ -72,7 +72,7 @@
         )
         branch = summed_on_arrival(projected, "tp", 1)
         return (own_cols + 0.5 * branch).astype(jnp.bfloat16)
-    branch = lax.psum(projected, "tp").astype(jnp.float32)
+    branch = jnp.sum(lax.all_gather(projected, "tp"), axis=0).astype(jnp.float32)
     return (as_float + 0.5 * branch).astype(jnp.bfloat16)
 
 

time: 231 us -> 221 us (0.957)
  blocking collectives: 156 us -> 143 us
  waiting for transfers between devices: 36.3 us -> 39.6 us
    psum x1 -> x0, blocking collectives: 23.5 us -> none  [feed_forward(): branch = lax.psum(projected, 'tp').astype(jnp.float32)]
    all_gather x0 -> x1, blocking collectives: none -> 16.2 us  [feed_forward(): lax.all_gather(projected, 'tp')]
    all_to_all x2, waiting for transfers between devices: 24.2 us -> 27.5 us  [summed_on_arrival(): lax.all_to_all(blocks, axis, split_axis=0, concat_axis=0, tiled=True)]
where the time goes in v1:
time: 221 us
  blocking collectives  143 us (65%)
  waiting for transfers between devices  39.6 us (18%)
  starting transfers between devices  20.9 us (9%)
  matrix products  7.7 us (3%)
  local copies, waits for them, and re-layouts  4.95 us (2%)
  other arithmetic  3.42 us (2%)
    all_to_all x2, blocking collectives, summed_on_arrival(): lax.all_to_all(blocks, axis, split_axis=0, concat_axis=0, tiled=True)  52.4 us
    all_to_all x2, blocking collectives, from_everyone(): return lax.all_to_all(copies, axis, split_axis=0, concat_axis=0, tiled=True)  34.7 us
    all_to_all x2, waiting for transfers between devices, summed_on_arrival(): lax.all_to_all(blocks, axis, split_axis=0, concat_axis=0, tiled=True)  27.5 us
    psum x1, blocking collectives, token_mixer(): branch = lax.psum(projected, 'tp').astype(jnp.float32)  23.8 us
    all_gather x1, blocking collectives, body(): columns = lax.all_gather(residual_in, 'tp', axis=1, tiled=True)  16.2 us
    all_gather x1, blocking collectives, feed_forward(): lax.all_gather(projected, 'tp')  16.2 us
    all_to_all x2, starting transfers between devices, summed_on_arrival(): lax.all_to_all(blocks, axis, split_axis=0, concat_axis=0, tiled=True)  15.3 us
    all_to_all x1, waiting for transfers between devices, from_everyone(): return lax.all_to_all(copies, axis, split_axis=0, concat_axis=0, tiled=True)  12.1 us
  transfers between devices with their start and end apart: 3, of which 3 were waited for; matrix products, arithmetic and copies ran while one was open for 0% of the time, Pallas kernels for 0%

profile of v1, /device:TPU:1, one launch (start us, length us, event | category | flops | bytes accessed | tf_op | source)
XLA Modules:
  0.0 220.8 jit_solution(6464711819197439719)
XLA Ops:
  0.6 16.2 %all_gather.9 = bf16[256,64]{0,1:T(8,128)(2,1)S(1)} all-gather(bf16[256,8]{0,1:T(8,128)(2,1)} %param.21), channel_id=1, replica_groups=mesh['kv'=32,'tp'=8] {'tp'}, dimensions={1}, use_global_device_ids=true | all-gather | bytes 36864 | tf_op jit(solution)/shard_map/all_gather | solution.py:195
  17.1 1.4 fusion
  18.6 31.3 %all_to_all.35 = bf16[32,8,1409]{2,1,0:T(8,128)(2,1)S(1)} all-to-all(bf16[32,8,1409]{2,1,0:T(8,128)(2,1)S(1)} %pad_maximum_fusion), channel_id=1, replica_groups=mesh['kv'=32,'tp'=8] {'kv'}, dimensions={0} | all-to-all | bytes 1442816 | tf_op jit(solution)/shard_map/all_to_all | solution.py:17
  50.2 0.8 broadcast_in_dim.10
  51.0 5.6 %all-to-all-start.1 = ((bf16[32,8,704]{2,1,0:T(8,128)(2,1)}), bf16[32,8,704]{2,1,0:T(8,128)(2,1)S(1)}, u32[]{:S(2)}, u32[]{:S(2)}) async-start(bf16[32,8,704]{2,1,0:T(8,128)(2,1)} %broadcast_in_dim.10), calls=%async_computation.1 | async-start | bytes 786432 | tf_op jit(solution)/shard_map/all_to_all | solution.py:40
  56.6 0.7 constant_dynamic-slice_fusion
  57.3 12.1 %all-to-all-done.1 = bf16[32,8,704]{2,1,0:T(8,128)(2,1)S(1)} async-done(((bf16[32,8,704]{2,1,0:T(8,128)(2,1)}), bf16[32,8,704]{2,1,0:T(8,128)(2,1)S(1)}, u32[]{:S(2)}, u32[]{:S(2)}) %all-to-all-start.1) | async-done | bytes 360480 | tf_op jit(solution)/shard_map/all_to_all | solution.py:40
  69.7 16.2 %all-gather = bf16[2048,64]{0,1:T(8,128)(2,1)S(1)} all-gather(bf16[256,64]{0,1:T(8,128)(2,1)S(1)} %convolution_convert_fusion.5), channel_id=2, replica_groups=mesh['kv'=32,'tp'=8] {'tp'}, dimensions={0}, use_global_device_ids=true | all-gather | bytes 294912 | tf_op jit(solution)/shard_map/all_gather | solution.py:75
  87.2 1.1 concatenate.39
  88.3 4.0 %all-to-all-start.2 = ((bf16[32,8,1545]{2,1,0:T(8,128)(2,1)}), bf16[32,8,1545]{2,1,0:T(8,128)(2,1)S(1)}, u32[]{:S(2)}, u32[]{:S(2)}) async-start(bf16[32,8,1545]{2,1,0:T(8,128)(2,1)} %concatenate.39), calls=%async_computation.2 | async-start | bytes 1703936 | tf_op jit(solution)/shard_map/all_to_all | solution.py:17
  92.3 22.8 %all-to-all-done.2 = bf16[32,8,1545]{2,1,0:T(8,128)(2,1)S(1)} async-done(((bf16[32,8,1545]{2,1,0:T(8,128)(2,1)}), bf16[32,8,1545]{2,1,0:T(8,128)(2,1)S(1)}, u32[]{:S(2)}, u32[]{:S(2)}) %all-to-all-start.2) | async-done | bytes 791072 | tf_op jit(solution)/shard_map/all_to_all | solution.py:17
  116.0 2.0 fusion.3
  118.1 0.7 multiply_add_fusion
  119.0 1.2 copy-done.2
  120.2 1.9 fusion.67
  122.3 15.9 %all_to_all.36 = bf16[32,8,512]{2,1,0:T(8,128)(2,1)S(1)} all-to-all(bf16[32,8,512]{2,1,0:T(8,128)(2,1)S(1)} %broadcast_in_dim.13), channel_id=1, replica_groups=mesh['kv'=32,'tp'=8] {'kv'}, dimensions={0} | all-to-all | bytes 524288 | tf_op jit(solution)/shard_map/all_to_all | solution.py:40
  138.4 23.8 %psum.7 = bf16[256,64]{0,1:T(8,128)(2,1)S(1)} all-reduce(bf16[256,64]{0,1:T(8,128)(2,1)S(1)} %convolution_convert_fusion.3), channel_id=1, replica_groups=mesh['kv'=32,'tp'=8] {'tp'}, use_global_device_ids=true, to_apply=%region_8.9 | all-reduce | flops 16384 | bytes 65536 | tf_op jit(solution)/shard_map/psum | solution.py:168
  162.6 0.5 fusion.2
  163.1 21.1 %all_to_all.37 = bf16[32,8,1409]{2,1,0:T(8,128)(2,1)S(1)} all-to-all(bf16[32,8,1409]{2,1,0:T(8,128)(2,1)S(1)} %pad_maximum_fusion.1), channel_id=1, replica_groups=mesh['kv'=32,'tp'=8] {'kv'}, dimensions={0} | all-to-all | bytes 1442816 | tf_op jit(solution)/shard_map/all_to_all | solution.py:17
  184.6 18.7 %all_to_all.38 = bf16[32,8,704]{2,1,0:T(8,128)(2,1)S(1)} all-to-all(bf16[32,8,704]{2,1,0:T(8,128)(2,1)S(1)} %broadcast_in_dim.14), channel_id=1, replica_groups=mesh['kv'=32,'tp'=8] {'kv'}, dimensions={0} | all-to-all | bytes 720896 | tf_op jit(solution)/shard_map/all_to_all | solution.py:40
  203.3 0.9 fusion.5
  204.2 11.3 %all-to-all-start.6 = ((bf16[8,256,8]{1,2,0:T(8,128)(2,1)}), bf16[8,256,8]{1,2,0:T(8,128)(2,1)S(1)}, u32[]{:S(2)}, u32[]{:S(2)}) async-start(bf16[8,256,8]{1,2,0:T(8,128)(2,1)} %fusion.5), calls=%async_computation.6 | async-start | bytes 65536 | tf_op jit(solution)/shard_map/all_to_all | solution.py:17
  215.5 4.7 %all-to-all-done.6 = bf16[8,256,8]{1,2,0:T(8,128)(2,1)S(1)} async-done(((bf16[8,256,8]{1,2,0:T(8,128)(2,1)}), bf16[8,256,8]{1,2,0:T(8,128)(2,1)S(1)}, u32[]{:S(2)}, u32[]{:S(2)}) %all-to-all-start.6) | async-done | bytes 32800 | tf_op jit(solution)/shard_map/all_to_all | solution.py:17
  220.2 0.6 add_convert_fusion
  (75 shorter events, 4.3 us)
Async XLA Ops:
  0.6 68.8 %copy-start = (bf16[704,64]{0,1:T(8,128)(2,1)S(1)}, bf16[704,64]{0,1:T(8,128)(2,1)}, u32[]{:S(2)}) copy-start(bf16[704,64]{0,1:T(8,128)(2,1)} %param.26) | copy-start | bytes 270340
  49.9 36.2 %copy-start.11 = (f32[64]{0:T(128)S(1)}, f32[64]{0:T(128)}, u32[]{:S(2)}) copy-start(f32[64]{0:T(128)} %param.27) | copy-start | bytes 772
  49.9 36.8 %copy-start.6 = (bf16[64,512]{1,0:T(8,128)(2,1)S(1)}, bf16[64,512]{1,0:T(8,128)(2,1)}, u32[]{:S(2)}) copy-start(bf16[64,512]{1,0:T(8,128)(2,1)} %param.31) | copy-start | bytes 196612
  49.9 36.8 %copy-start.7 = (bf16[64,512]{1,0:T(8,128)(2,1)S(1)}, bf16[64,512]{1,0:T(8,128)(2,1)}, u32[]{:S(2)}) copy-start(bf16[64,512]{1,0:T(8,128)(2,1)} %param.30) | copy-start | bytes 196612
  49.9 36.8 %copy-start.9 = (bf16[64,256]{1,0:T(8,128)(2,1)S(1)}, bf16[64,256]{1,0:T(8,128)(2,1)}, u32[]{:S(2)}) copy-start(bf16[64,256]{1,0:T(8,128)(2,1)} %param.29) | copy-start | bytes 98308
  49.9 36.8 %copy-start.10 = (bf16[64,256]{1,0:T(8,128)(2,1)S(1)}, bf16[64,256]{1,0:T(8,128)(2,1)}, u32[]{:S(2)}) copy-start(bf16[64,256]{1,0:T(8,128)(2,1)} %param.28) | copy-start | bytes 98308
  51.0 18.4 %all-to-all-start.1 = ((bf16[32,8,704]{2,1,0:T(8,128)(2,1)}), bf16[32,8,704]{2,1,0:T(8,128)(2,1)S(1)}, u32[]{:S(2)}, u32[]{:S(2)}) async-start(bf16[32,8,704]{2,1,0:T(8,128)(2,1)} %broadcast_in_dim.10), calls=%async_computation.1 | async-start | bytes 786432 | tf_op jit(solution)/shard_map/all_to_all | solution.py:40
  86.7 5.6 %copy-start.15 = (f32[4]{0:T(128)S(1)}, f32[4]{0:T(128)}, u32[]{:S(2)}) copy-start(f32[4]{0:T(128)} %param.34) | copy-start | bytes 52
  87.2 28.5 %copy-start.14 = (f32[4]{0:T(128)S(1)}, f32[4]{0:T(128)}, u32[]{:S(2)}) copy-start(f32[4]{0:T(128)} %param.35) | copy-start | bytes 52
  87.2 28.8 %copy-start.1 = (f32[8,4,128,128]{3,2,1,0:T(8,128)S(1)}, f32[8,4,128,128]{3,2,1,0:T(8,128)}, u32[]{:S(2)}) copy-start(f32[8,4,128,128]{3,2,1,0:T(8,128)} %param.22) | copy-start | bytes 6291460
  88.3 26.8 %all-to-all-start.2 = ((bf16[32,8,1545]{2,1,0:T(8,128)(2,1)}), bf16[32,8,1545]{2,1,0:T(8,128)(2,1)S(1)}, u32[]{:S(2)}, u32[]{:S(2)}) async-start(bf16[32,8,1545]{2,1,0:T(8,128)(2,1)} %concatenate.39), calls=%async_computation.2 | async-start | bytes 1703936 | tf_op jit(solution)/shard_map/all_to_all | solution.py:17
  118.9 1.3 copy-start.2
  118.9 3.3 %copy-start.13 = (f32[128]{0:T(128)S(1)}, f32[128]{0:T(128)}, u32[]{:S(2)}) copy-start(f32[128]{0:T(128)} %param.36) | copy-start | bytes 1540
  118.9 19.3 %copy-start.8 = (bf16[512,64]{0,1:T(8,128)(2,1)S(1)}, bf16[512,64]{0,1:T(8,128)(2,1)}, u32[]{:S(2)}) copy-start(bf16[512,64]{0,1:T(8,128)(2,1)} %param.37) | copy-start | bytes 196612
  118.9 43.6 %copy-start.3 = (bf16[64,704]{1,0:T(8,128)(2,1)S(1)}, bf16[64,704]{1,0:T(8,128)(2,1)}, u32[]{:S(2)}) copy-start(bf16[64,704]{1,0:T(8,128)(2,1)} %param.40) | copy-start | bytes 270340
  118.9 43.6 %copy-start.4 = (bf16[64,704]{1,0:T(8,128)(2,1)S(1)}, bf16[64,704]{1,0:T(8,128)(2,1)}, u32[]{:S(2)}) copy-start(bf16[64,704]{1,0:T(8,128)(2,1)} %param.39) | copy-start | bytes 270340
  118.9 43.6 %copy-start.12 = (f32[64]{0:T(128)S(1)}, f32[64]{0:T(128)}, u32[]{:S(2)}) copy-start(f32[64]{0:T(128)} %param.38) | copy-start | bytes 772
  163.1 40.2 %copy-start.5 = (bf16[704,64]{0,1:T(8,128)(2,1)S(1)}, bf16[704,64]{0,1:T(8,128)(2,1)}, u32[]{:S(2)}) copy-start(bf16[704,64]{0,1:T(8,128)(2,1)} %param.41) | copy-start | bytes 270340
  204.2 16.0 %all-to-all-start.6 = ((bf16[8,256,8]{1,2,0:T(8,128)(2,1)}), bf16[8,256,8]{1,2,0:T(8,128)(2,1)S(1)}, u32[]{:S(2)}, u32[]{:S(2)}) async-start(bf16[8,256,8]{1,2,0:T(8,128)(2,1)} %fusion.5), calls=%async_computation.6 | async-start | bytes 65536 | tf_op jit(solution)/shard_map/all_to_all | solution.py:17
